TPU v7x, 32 devices: a whole 2x2x4 slice. The times are simulated.
32 devices in a mesh: sp: 8 (over z, y), tp: 4 (over x, core).
Axes of the slice: x: 2, y: 2, z: 4, core: 2. Of those that a mesh axis runs over, the one named last changes fastest.
Arguments:
- tokens: bfloat16 [4096, 2048], P('sp'), may hold values from -24 to 24
- w_query: bfloat16 [2048, 1536], P('sp', 'tp'), as said below
- w_key: bfloat16 [2048, 1536], P('sp', 'tp'), as said below
- w_value: bfloat16 [2048, 1536], P('sp', 'tp'), may hold values from -0.125 to 0.125
- w_out: bfloat16 [512, 2048], P('tp', 'sp'), may hold values from -1.5 to 1.5
Outputs:
- mixed: bfloat16 [4096, 2048], P(('sp', 'tp'))
Inputs may be any that keep to these rules, and one draw needn't show every extreme that they name: `w_query`: every entry lies within 4 / sqrt(2048) of zero. `w_key`: every entry lies within 4 / sqrt(2048) of zero.
All inputs are finite; a program needn't handle non-finite values.
Results may differ from a plain program's by a relative error of at most 0.025.
Values may be sent and summed in bfloat16 or wider, within the bound.
A program may use at most 64 MiB of HBM per device.

v0:
```python
import functools
import math

import jax
import jax.numpy as jnp
import numpy as np
from jax import lax
from jax.experimental import pallas as pl
from jax.experimental.pallas import tpu as pltpu
from jax.sharding import PartitionSpec as P

GROUPS = 3
DH = 128
WIN1 = 128
WIN2 = 512
WIN3 = 2048
SECOND_DILATION = 4
THIRD_DILATION = 16


ROPE_BASE = 500000.0


def from_behind(block, axis, distance):
    devices = range(lax.axis_size(axis))
    route = [(i - distance, i) for i in devices if i - distance in devices]
    return lax.ppermute(block, axis, route)


def rotate(projected, offset):
    tok_rows = projected.shape[0]
    head_size = projected.shape[-1]
    half_size = head_size // 2
    positions = (offset + jnp.arange(tok_rows, dtype=jnp.int32)).astype(jnp.float32)
    frequency = 1.0 / ROPE_BASE ** (jnp.arange(0, head_size, 2, dtype=jnp.float32) / head_size)
    angles = (positions[:, None] * frequency[None, :]).reshape(tok_rows, 1, 1, half_size)
    cosine = jnp.cos(angles)
    sine_part = jnp.sin(angles)
    first_half = projected[..., :half_size]
    second_half = projected[..., half_size:]
    return jnp.concatenate(
        [
            first_half * cosine - second_half * sine_part,
            second_half * cosine + first_half * sine_part,
        ],
        axis=-1,
    )


def window_attend(query_part, buffer, steps, stride, offset):
    tok_rows, heads_here, head_size = query_part.shape
    sub_rows = tok_rows // stride
    key_rows = buffer.shape[1] // stride
    query_sub = query_part.reshape(sub_rows, stride, heads_here, head_size).transpose(1, 2, 0, 3)
    pair_sub = buffer.reshape(2, key_rows, stride, heads_here, head_size).transpose(0, 2, 3, 1, 4)
    block_rows = math.gcd(sub_rows, steps) if sub_rows > steps else sub_rows
    block_list = sub_rows // block_rows
    query_blocks = query_sub.reshape(stride, heads_here, block_list, block_rows, head_size)
    key_blocks = jnp.stack(
        [
            pair_sub[:, :, :, index * block_rows : index * block_rows + block_rows + steps]
            for index in range(block_list)
        ],
        axis=3,
    )
    scores = jnp.einsum(
        "zhnqe,zhnke->zhnqk", query_blocks, key_blocks[0], preferred_element_type=jnp.float32
    ) * head_size ** (-0.5)
    query_index = (jnp.arange(block_list, dtype=jnp.int32) * block_rows)[
        :, None, None
    ] + jnp.arange(block_rows, dtype=jnp.int32)[None, :, None]
    key_index = (jnp.arange(block_list, dtype=jnp.int32) * block_rows)[:, None, None] + jnp.arange(
        block_rows + steps, dtype=jnp.int32
    )[None, None, :]
    spacing = query_index + steps - key_index
    residue = jnp.arange(stride, dtype=jnp.int32)[:, None, None, None]
    key_position = offset + (key_index[None] - steps) * stride + residue
    allowed = (spacing[None] >= 0) & (spacing[None] <= steps) & (key_position >= 0)
    scores = jnp.where(allowed[:, None], scores, -jnp.inf)
    row_max = jnp.max(scores, axis=-1)
    exponent = jnp.exp(scores - row_max[..., None])
    totals = jnp.sum(exponent, axis=-1)
    probs = (exponent / totals[..., None]).astype(jnp.bfloat16)
    mixed = jnp.einsum(
        "zhnqk,zhnke->zhnqe", probs, key_blocks[1], preferred_element_type=jnp.float32
    )
    mixed = mixed.reshape(stride, heads_here, sub_rows, head_size).transpose(2, 0, 1, 3)
    log_total = (row_max + jnp.log(totals)).reshape(stride, heads_here, sub_rows).transpose(2, 0, 1)
    return (mixed.reshape(tok_rows, heads_here, head_size), log_total.reshape(tok_rows, heads_here))


def reach_back(key_value, distance_max):
    tok_rows = key_value.shape[1]
    gathered = key_value
    pieces_held = 1
    while pieces_held < distance_max + 1:
        slice_share = min(pieces_held, distance_max + 1 - pieces_held)
        arrived = from_behind(
            gathered[:, gathered.shape[1] - slice_share * tok_rows :], "sp", pieces_held
        )
        gathered = jnp.concatenate([arrived, gathered], axis=1)
        pieces_held = pieces_held + slice_share
    return gathered


def on_device(tokens, w_query, w_key, w_value, w_out):
    tok_rows = tokens.shape[0]
    heads_here = w_out.shape[0] // DH
    offset = lax.axis_index("sp") * tok_rows
    weight_parts = (
        lax.all_gather(w_query, "sp", axis=0, tiled=True),
        lax.all_gather(w_key, "sp", axis=0, tiled=True),
        lax.all_gather(w_value, "sp", axis=0, tiled=True),
    )
    query_raw, key_raw, value_raw = tuple(
        (
            jnp.dot(tokens, weight_rows, preferred_element_type=jnp.float32)
            for weight_rows in weight_parts
        )
    )
    head_shape = (tok_rows, heads_here, GROUPS, DH)
    queries = rotate(query_raw.reshape(head_shape), offset).astype(jnp.bfloat16)
    keys_all = rotate(key_raw.reshape(head_shape), offset).astype(jnp.bfloat16)
    values_all = value_raw.astype(jnp.bfloat16).reshape(head_shape)
    windows = (WIN1, WIN2, WIN3)
    step_sizes = (1, SECOND_DILATION, THIRD_DILATION)
    outputs = []
    log_totals = []
    for group_index in range(GROUPS):
        key_value = jnp.stack([keys_all[:, :, group_index], values_all[:, :, group_index]])
        key_value = key_value.reshape(2, tok_rows, heads_here * DH)
        window = windows[group_index]
        if group_index == 0:
            near_rows = from_behind(key_value[:, tok_rows - window :], "sp", 1)
            buffer = jnp.concatenate([near_rows, key_value], axis=1)
        else:
            distance_max = (window + tok_rows - 1) // tok_rows
            buffer = reach_back(key_value, distance_max)
        group_out, log_total = window_attend(
            queries[:, :, group_index],
            buffer,
            window // step_sizes[group_index],
            step_sizes[group_index],
            offset,
        )
        outputs.append(group_out)
        log_totals.append(log_total)
    group_weights = jax.nn.softmax(jnp.stack(log_totals), axis=0)
    merged = jnp.sum(group_weights[..., None] * jnp.stack(outputs), axis=0).astype(jnp.bfloat16)
    merged = merged.reshape(tok_rows, heads_here * DH)
    w_whole = lax.all_gather(w_out, "sp", axis=1, tiled=True)
    return lax.psum_scatter(
        jnp.dot(merged, w_whole, preferred_element_type=jnp.float32).astype(jnp.bfloat16),
        "tp",
        scatter_dimension=0,
        tiled=True,
    )


def layer_kernel(
    nz,
    tokens, w_key, w_value, w_query, w_out, freq, out,
    weights, tok_in, tok_turned, cosine, sine, queries, pair0, send1, near1, far2,
    out_rows, mine, heads_in, got01, top01, sum01,
    swap_s, tok_r, w_r, up_s, down_s, side_s, o_r, o_s, o_r2, far_s, far_r, near_s, near_r, head_s, head_r,
):
    tok_rows, depth = tokens.shape
    k_rows, cols = w_key.shape
    sub = tok_rows // THIRD_DILATION
    sub_log = sub.bit_length() - 1
    block = tok_rows // SECOND_DILATION
    tail = WIN1
    sp, tp = lax.axis_index("sp"), lax.axis_index("tp")
    z, y = sp // 2, sp % 2
    x, c = tp // 2, tp % 2
    rank = 2 * z + c
    side = (sp, 2 * x + 1 - c)
    above = (sp + 2, tp)
    below = (sp - 2, tp)
    partner = (2 * z + 1 - y, 2 * x + 1 - c)
    stays = c == y
    has_up, has_down = z < nz - 1, z > 0

    def send(src, dst, s_sem, r_sem, where):
        return pltpu.make_async_remote_copy(
            src_ref=src, dst_ref=dst, send_sem=s_sem, recv_sem=r_sem,
            device_id=where, device_id_type=pl.DeviceIdType.MESH,
        )

    barrier = pltpu.get_barrier_semaphore()

    def greet(where):
        pl.semaphore_signal(barrier, inc=1, device_id=where, device_id_type=pl.DeviceIdType.MESH)

    for dy in range(2):
        for dx in range(2):
            for dc in range(2):
                if dy + dx + dc:
                    greet((2 * z + (y + dy) % 2, 2 * ((x + dx) % 2) + (c + dc) % 2))
    pl.when(has_up)(lambda: greet(above))
    pl.when(has_down)(lambda: greet(below))
    pl.when(has_up & (c == 1))(lambda: greet((sp + 2, 2 * x)))
    pl.when(has_down & (c == 0))(lambda: greet((sp - 2, 2 * x + 1)))
    greeters = 7 + jnp.where(has_up, 1 + c, 0) + jnp.where(has_down, 2 - c, 0)
    pl.semaphore_wait(barrier, greeters)

    parts = (w_key, w_value, w_query)

    def chunk(a, s):
        return weights.at[a, pl.ds(pl.multiple_of(s * k_rows, k_rows), k_rows), :]

    def o_chunk(zz):
        return out_rows.at[c, x, y, zz]

    def swapped(a):
        there = 2 * z + 1 - c
        return send(parts[a], chunk(a, there), swap_s.at[a], w_r.at[a, there], partner)

    def tok_swapped():
        return send(tokens, tok_in, swap_s.at[3], tok_r, partner)

    def kept(a):
        return pltpu.make_async_copy(parts[a], chunk(a, rank), w_r.at[a, rank])

    def o_kept():
        return pltpu.make_async_copy(w_out, o_chunk(z), o_r.at[z])

    @pl.when(stays)
    def _():
        for a in range(3):
            kept(a).start()

    @pl.when(jnp.logical_not(stays))
    def _():
        swapped(0).start()
        swapped(1).start()
        tok_swapped().start()
        swapped(2).start()

    o_kept().start()

    def go(a, zz, kind):
        s = 2 * zz + c
        ref = chunk(a, s) if a < 3 else o_chunk(zz)
        r_sem = w_r.at[a, s] if a < 3 else o_r.at[zz]
        s_sem = {"up": up_s, "down": down_s, "side": side_s}[kind].at[a, zz]
        return send(ref, ref, s_sem, r_sem, {"up": above, "down": below, "side": side}[kind])

    def own(a):
        if a < 3:
            pl.when(stays)(lambda: kept(a).wait())
            pl.when(jnp.logical_not(stays))(lambda: go(a, z, "side").wait_recv())
        else:
            o_kept().wait()
        pl.when(has_up)(lambda: go(a, z, "up").start())
        pl.when(has_down)(lambda: go(a, z, "down").start())
        if a < 3:
            go(a, z, "side").start()

    def relay(a, d):
        @pl.when(z - d >= 0)
        def _():
            go(a, z - d, "up").wait_recv()
            pl.when(has_up)(lambda: go(a, z - d, "up").start())
            if a < 3:
                go(a, z - d, "side").start()

        @pl.when(z + d < nz)
        def _():
            go(a, z + d, "down").wait_recv()
            pl.when(has_down)(lambda: go(a, z + d, "down").start())
            if a < 3:
                go(a, z + d, "side").start()

    def others(a):
        for zz in range(nz):
            s = 2 * zz + 1 - c
            send(chunk(a, s), chunk(a, s), side_s.at[a, zz], w_r.at[a, s], side).wait_recv()

    def row_time(p):
        b, i = p >> sub_log, p & (sub - 1)
        return THIRD_DILATION * i + (b >> 2) + SECOND_DILATION * (b & 3)

    def tail_time(u):
        per = tail // THIRD_DILATION
        b, i = u >> (per.bit_length() - 1), u & (per - 1)
        return THIRD_DILATION * (sub - per + i) + (b >> 2) + SECOND_DILATION * (b & 3) - tok_rows

    own(0)
    own(1)

    def angles(index, carry):
        rows = pl.ds(pl.multiple_of(index * block, block), block)
        p = lax.broadcasted_iota(jnp.int32, (block, DH), 0) + index * block
        angle = (row_time(p) + rank * tok_rows).astype(jnp.float32) * freq[...]
        lane = lax.broadcasted_iota(jnp.int32, (block, DH), 1)
        cosine[rows, :] = jnp.cos(angle)
        turned = jnp.sin(angle)
        sine[rows, :] = jnp.where(lane < DH // 2, -turned, turned)
        return carry

    lax.fori_loop(0, SECOND_DILATION, angles, 0)

    def relay_all(a, following):
        for d in range(1, nz):
            if d == nz - 1 and following is not None:
                own(following)
            relay(a, d)

    def order(source):
        p = row_time(lax.broadcasted_iota(jnp.int32, (tok_rows, tok_rows), 0))
        t = lax.broadcasted_iota(jnp.int32, (tok_rows, tok_rows), 1)
        pick = jnp.where(p == t, 1.0, 0.0).astype(jnp.bfloat16)

        def piece(index, carry):
            at = pl.ds(pl.multiple_of(index * 256, 256), 256)
            tok_turned[:, at] = jnp.dot(
                pick, source[:, at], preferred_element_type=jnp.float32
            ).astype(jnp.bfloat16)
            return carry

        lax.fori_loop(0, depth // 256, piece, 0)

    pl.when(stays)(lambda: order(tokens))

    def o_y():
        return send(out_rows.at[c, x, y], out_rows.at[c, x, y], o_s.at[0], o_r2.at[0], (2 * z + 1 - y, tp))

    def o_x():
        return send(out_rows.at[c, x], out_rows.at[c, x], o_s.at[1], o_r2.at[1], (sp, 2 * (1 - x) + c))

    def o_c():
        return send(out_rows.at[c], out_rows.at[c], o_s.at[2], o_r2.at[2], side)

    relay_all(0, 3)
    relay_all(3, None)
    o_y().start()
    relay_all(1, 2)
    relay(2, 1)

    @pl.when(jnp.logical_not(stays))
    def _():
        tok_swapped().wait_recv()
        order(tok_in)

    def project(a, store):
        def piece(index, carry):
            rows = pl.ds(pl.multiple_of(index * block, block), block)
            raw = jnp.dot(tok_turned[rows, :], weights[a], preferred_element_type=jnp.float32)
            for g in range(GROUPS):
                part = raw[:, g * DH : (g + 1) * DH]
                if a != 1:
                    part = part * cosine[rows, :] + pltpu.roll(part, DH // 2, 1) * sine[rows, :]
                store(index, rows, g, part)
            return carry

        lax.fori_loop(0, SECOND_DILATION, piece, 0)

    def keep_pair(which):
        def store(index, rows, g, part):
            if g == 2:
                far2[0, which, rows, :] = part.astype(jnp.bfloat16)
            elif g == 1:
                send1[which, rows, :] = part.astype(jnp.bfloat16)
            else:
                pair0[which, rows, :] = part.astype(jnp.bfloat16)
                per = tail // THIRD_DILATION
                last = jnp.concatenate(
                    [part[b * sub + sub - per : (b + 1) * sub] for b in range(4)], axis=0
                )
                at = pl.ds(pl.multiple_of(tok_rows + index * 4 * per, 4 * per), 4 * per)
                send1[which, at, :] = last.astype(jnp.bfloat16)

        return store

    others(0)
    project(0, keep_pair(0))
    others(1)
    project(1, keep_pair(1))

    def far(index, src, dst, where):
        return send(far2.at[src], far2.at[dst], far_s.at[index], far_r.at[dst], where)

    def near(where):
        return send(send1, near1, near_s, near_r, where)

    up_other = (sp + 2, 2 * x)
    pl.when(has_up)(lambda: far(0, 0, 2, above).start())
    pl.when(c == 0)(lambda: far(1, 0, 1, side).start())
    pl.when(c == 0)(lambda: near(side).start())
    pl.when(has_up & (c == 1))(lambda: near(up_other).start())

    for d in range(1, 5):
        @pl.when(rank < d)
        def _(d=d):
            far2[d] = jnp.zeros(far2.shape[1:], far2.dtype)

    @pl.when(rank < 1)
    def _():
        near1[...] = jnp.zeros(near1.shape, near1.dtype)

    for d in range(2, nz):
        relay(2, d)
    @pl.when(has_down)
    def _():
        far(0, 0, 2, above).wait_recv()
        pl.when(has_up)(lambda: far(2, 2, 4, above).start())
        pl.when(c == 0)(lambda: far(3, 2, 3, side).start())
        pl.when(c == 1)(lambda: far(3, 2, 1, side).start())

    o_y().wait()
    o_x().start()
    others(2)

    def keep_query(index, rows, g, part):
        queries[g, rows, :] = part.astype(jnp.bfloat16)

    project(2, keep_query)

    scale = DH ** (-0.5)
    far_off = 1 << 24

    def dots(q, k):
        return lax.dot_general(q, k, (((1,), (1,)), ((), ())), preferred_element_type=jnp.float32)

    def iota(shape, axis):
        return lax.broadcasted_iota(jnp.int32, shape, axis)

    def soft(scores, time_q, time_k, reach, first):
        gap = time_q - jnp.where(time_k >= first, time_k, far_off)
        scores = jnp.where((gap >= 0) & (gap <= reach), scores * scale, -jnp.inf)
        top = jnp.max(scores, axis=-1, keepdims=True)
        weight = jnp.exp(scores - top)
        return top, jnp.sum(weight, axis=-1, keepdims=True), weight.astype(jnp.bfloat16)

    def near_groups(index, carry):
        begin = index * block
        rows = pl.ds(pl.multiple_of(begin, block), block)
        q = queries[0, rows, :]
        tails = pl.ds(tok_rows, tail)
        scores = jnp.concatenate([dots(q, near1[0, tails, :]), dots(q, pair0[0])], axis=1)
        lane = iota((1, tail + tok_rows), 1)
        time_k = jnp.where(lane < tail, tail_time(lane & (tail - 1)), row_time(lane - tail))
        time_q = row_time(iota((block, 1), 0) + begin)
        top0, sum0, weight = soft(scores, time_q, time_k, WIN1, -rank * tok_rows)
        got0 = jnp.dot(weight[:, :tail], near1[1, tails, :], preferred_element_type=jnp.float32)
        got0 += jnp.dot(weight[:, tail:], pair0[1], preferred_element_type=jnp.float32)
        q = queries[1, rows, :]
        scores = jnp.concatenate([dots(q, near1[0, rows, :]), dots(q, send1[0, rows, :])], axis=1)

        def step_of(place):
            return 4 * (place & (sub - 1)) + (place >> sub_log)

        lane = iota((1, 2 * block), 1)
        step_k = step_of(lane & (block - 1)) + jnp.where(lane < block, -block, 0)
        top1, sum1, weight = soft(
            scores, step_of(iota((block, 1), 0)), step_k, WIN2 // SECOND_DILATION, -rank * block
        )
        got1 = jnp.dot(weight[:, :block], near1[1, rows, :], preferred_element_type=jnp.float32)
        got1 += jnp.dot(weight[:, block:], send1[1, rows, :], preferred_element_type=jnp.float32)
        top = jnp.maximum(top0, top1)
        f0, f1 = jnp.exp(top0 - top), jnp.exp(top1 - top)
        got01[rows, :] = f0 * got0 + f1 * got1
        top01[rows, :] = top
        sum01[rows, :] = f0 * sum0 + f1 * sum1
        return carry

    def far_group(index, carry):
        begin = index * block
        rows = pl.ds(pl.multiple_of(begin, block), block)
        all_scores = []
        for b in range(4):
            here = pl.ds(pl.multiple_of(begin + b * sub, sub), sub)
            keys = jnp.concatenate([far2[d, 0, here, :] for d in (4, 3, 2, 1, 0)], axis=0)
            all_scores.append(dots(queries[2, here, :], keys))
        scores = jnp.concatenate(all_scores, axis=0)
        step_q = iota((block, 1), 0) & (sub - 1)
        step_k = iota((1, 5 * sub), 1) - 4 * sub
        top2, sum2, weight = soft(scores, step_q, step_k, WIN3 // THIRD_DILATION, -rank * sub)
        got = []
        for b in range(4):
            here = pl.ds(pl.multiple_of(begin + b * sub, sub), sub)
            vals = jnp.concatenate([far2[d, 1, here, :] for d in (4, 3, 2, 1, 0)], axis=0)
            got.append(jnp.dot(weight[b * sub : (b + 1) * sub], vals, preferred_element_type=jnp.float32))
        got2 = jnp.concatenate(got, axis=0)
        top1 = top01[rows, :]
        top = jnp.maximum(top1, top2)
        f1, f2 = jnp.exp(top1 - top), jnp.exp(top2 - top)
        total = f1 * sum01[rows, :] + f2 * sum2
        mine[0, rows, :] = ((f1 * got01[rows, :] + f2 * got2) / total).astype(jnp.bfloat16)
        return carry

    pl.when(rank >= 1)(lambda: near(side).wait_recv())
    lax.fori_loop(0, SECOND_DILATION, near_groups, 0)
    o_x().wait()
    o_c().start()

    @pl.when(z >= 2)
    def _():
        far(2, 2, 4, above).wait_recv()
        pl.when(c == 1)(lambda: far(4, 4, 3, side).start())

    pl.when(rank >= 1)(lambda: far(1, 0, 1, side).wait_recv())
    pl.when(rank >= 3)(lambda: far(4, 4, 3, side).wait_recv())
    lax.fori_loop(0, SECOND_DILATION, far_group, 0)

    t = iota((tok_rows, tok_rows), 0)
    p = row_time(iota((tok_rows, tok_rows), 1))
    mine[1] = jnp.dot(
        jnp.where(p == t, 1.0, 0.0).astype(jnp.bfloat16), mine[0], preferred_element_type=jnp.float32
    ).astype(jnp.bfloat16)
    head = 2 * x + y
    quarter = tok_rows // 4

    def deal(k):
        return send(mine.at[1, pl.ds(k * quarter, quarter), :], heads_in.at[head], head_s.at[k], head_r.at[head], (2 * z + c, k))

    def deal_self(k):
        return pltpu.make_async_copy(mine.at[1, pl.ds(k * quarter, quarter), :], heads_in.at[head], head_r.at[head])

    for k in range(4):
        self_here = (y == c) & (tp == k)
        pl.when(self_here)(lambda k=k: deal_self(k).start())
        pl.when(jnp.logical_not(self_here))(lambda k=k: deal(k).start())

    o_c().wait()
    for h in range(4):
        pltpu.make_async_copy(heads_in.at[h], heads_in.at[h], head_r.at[h]).wait()
    for zz in range(nz):
        for yy in range(2):
            acc = None
            for h in range(4):
                one = jnp.dot(heads_in[h], out_rows[h % 2, h // 2, yy, zz], preferred_element_type=jnp.float32)
                acc = one if acc is None else acc + one
            width = w_out.shape[1]
            s = 2 * zz + yy
            out[:, s * width : (s + 1) * width] = acc.astype(jnp.bfloat16)

    for k in range(4):
        self_here = (y == c) & (tp == k)
        pl.when(jnp.logical_not(self_here))(lambda k=k: deal(k).wait_send())

    @pl.when(jnp.logical_not(stays))
    def _():
        for a in range(3):
            swapped(a).wait_send()
        tok_swapped().wait_send()

    for a in range(4):
        for zz in range(nz):
            pl.when(has_up & (zz <= z))(lambda a=a, zz=zz: go(a, zz, "up").wait_send())
            pl.when(has_down & (zz >= z))(lambda a=a, zz=zz: go(a, zz, "down").wait_send())
            if a < 3:
                go(a, zz, "side").wait_send()
    pl.when(has_up)(lambda: far(0, 0, 2, above).wait_send())
    pl.when(c == 0)(lambda: far(1, 0, 1, side).wait_send())
    pl.when((c == 0) | has_up)(lambda: near(side).wait_send())
    pl.when(has_down & has_up)(lambda: far(2, 2, 4, above).wait_send())
    pl.when(has_down)(lambda: far(3, 2, 3, side).wait_send())
    pl.when((z >= 2) & (c == 1))(lambda: far(4, 4, 3, side).wait_send())


def fits_kernel(n_sp, n_tp, tokens, w_query, w_out):
    tok_rows, depth = tokens.shape
    return (
        n_sp % 2 == 0
        and n_tp == 4
        and w_query.shape[1] == GROUPS * DH
        and w_out.shape[0] == DH
        and w_out.shape[1] % 128 == 0
        and w_query.shape[0] % 16 == 0
        and tok_rows == WIN2
        and 4 * tok_rows == WIN3
        and 4 * WIN1 == tok_rows
    )


def one_kernel(n_sp, tokens, w_query, w_key, w_value, w_out):
    nz = n_sp // 2
    tok_rows, depth = tokens.shape
    cols = w_query.shape[1]
    half = 1.0 / ROPE_BASE ** (np.arange(0, DH, 2) / DH)
    freq = jnp.asarray(np.concatenate([half, half]).reshape(1, DH), jnp.float32)
    bf, dma = jnp.bfloat16, pltpu.SemaphoreType.DMA
    return pl.pallas_call(
        functools.partial(layer_kernel, nz),
        out_shape=jax.ShapeDtypeStruct((tok_rows // 4, w_out.shape[1] * n_sp), bf),
        in_specs=[pl.BlockSpec(memory_space=pltpu.VMEM)] * 6,
        out_specs=pl.BlockSpec(memory_space=pltpu.VMEM),
        scratch_shapes=[
            pltpu.VMEM((3, depth, cols), bf),
            pltpu.VMEM((tok_rows, depth), bf),
            pltpu.VMEM((tok_rows, depth), bf),
            pltpu.VMEM((tok_rows, DH), jnp.float32),
            pltpu.VMEM((tok_rows, DH), jnp.float32),
            pltpu.VMEM((GROUPS, tok_rows, DH), bf),
            pltpu.VMEM((2, tok_rows, DH), bf),
            pltpu.VMEM((2, tok_rows + WIN1, DH), bf),
            pltpu.VMEM((2, tok_rows + WIN1, DH), bf),
            pltpu.VMEM((5, 2, tok_rows, DH), bf),
            pltpu.VMEM((2, 2, 2, nz, *w_out.shape), bf),
            pltpu.VMEM((2, tok_rows, DH), bf),
            pltpu.VMEM((4, tok_rows // 4, DH), bf),
            pltpu.VMEM((tok_rows, DH), jnp.float32),
            pltpu.VMEM((tok_rows, 1), jnp.float32),
            pltpu.VMEM((tok_rows, 1), jnp.float32),
            dma((4,)), dma, dma((3, n_sp)),
            dma((4, nz)), dma((4, nz)), dma((3, nz)),
            dma((nz,)), dma((3,)), dma((3,)),
            dma((5,)), dma((5,)), dma, dma,
            dma((4,)), dma((4,)),
        ],
        compiler_params=pltpu.CompilerParams(
            collective_id=0, has_side_effects=True, vmem_limit_bytes=32 * 1024 * 1024
        ),
    )(tokens, w_key, w_value, w_query, w_out, freq)


def on_mesh(n_sp, n_tp, *operands):
    tokens, w_query, _, _, w_out = operands
    if fits_kernel(n_sp, n_tp, tokens, w_query, w_out):
        return one_kernel(n_sp, *operands)
    return on_device(*operands)


def solution(mesh):
    placed = (P("sp", None), P("sp", "tp"), P("sp", "tp"), P("sp", "tp"), P("tp", "sp"))
    body = functools.partial(on_mesh, mesh.shape["sp"], mesh.shape["tp"])
    return jax.shard_map(
        body, mesh=mesh, in_specs=placed, out_specs=P(("sp", "tp"), None), check_vma=False
    )
```

profile of v0, /device:TPU:25, one launch (start us, length us, event | category | flops | bytes accessed | tf_op | source)
XLA Modules:
  0.0 83.7 jit_solution(3143800255113355664)
XLA Ops:
  0.0 0.0 copy-start
  0.0 1.6 %copy-done = bf16[512,2048]{1,0:T(8,128)(2,1)S(1)} copy-done((bf16[512,2048]{1,0:T(8,128)(2,1)S(1)}, bf16[512,2048]{1,0:T(8,128)(2,1)}, u32[]{:S(2)}) %copy-start) | copy-done | bytes 2097176
  1.6 0.0 copy-start.1
  1.6 0.9 %copy-done.1 = bf16[256,384]{1,0:T(8,128)(2,1)S(1)} copy-done((bf16[256,384]{1,0:T(8,128)(2,1)S(1)}, bf16[256,384]{1,0:T(8,128)(2,1)}, u32[]{:S(2)}) %copy-start.1) | copy-done | bytes 196632
  2.5 0.0 copy-start.2
  2.5 0.9 %copy-done.2 = bf16[256,384]{1,0:T(8,128)(2,1)S(1)} copy-done((bf16[256,384]{1,0:T(8,128)(2,1)S(1)}, bf16[256,384]{1,0:T(8,128)(2,1)}, u32[]{:S(2)}) %copy-start.2) | copy-done | bytes 196632
  3.4 0.0 copy-start.3
  3.4 0.9 %copy-done.3 = bf16[256,384]{1,0:T(8,128)(2,1)S(1)} copy-done((bf16[256,384]{1,0:T(8,128)(2,1)S(1)}, bf16[256,384]{1,0:T(8,128)(2,1)}, u32[]{:S(2)}) %copy-start.3) | copy-done | bytes 196632
  4.4 0.0 copy-start.4
  4.4 0.8 %copy-done.4 = bf16[128,256]{1,0:T(8,128)(2,1)S(1)} copy-done((bf16[128,256]{1,0:T(8,128)(2,1)S(1)}, bf16[128,256]{1,0:T(8,128)(2,1)}, u32[]{:S(2)}) %copy-start.4) | copy-done | bytes 65560
  5.2 0.0 copy-start.5
  5.2 0.7 copy-done.5
  5.9 77.0 %shard_map.64 = bf16[128,2048]{1,0:T(8,128)(2,1)S(1)} custom-call(bf16[512,2048]{1,0:T(8,128)(2,1)S(1)} %copy-done, bf16[256,384]{1,0:T(8,128)(2,1)S(1)} %copy-done.1, bf16[256,384]{1,0:T(8,128)(2,1)S(1)} %copy-done.2, bf16[256,384]{1,0:T(8,128)(2,1)S(1)} %copy-done.3, bf16[128,256]{1,0:T(8,128)(2,1)S(1)} %copy-done.4, f32[1,128]{1,0:T(1,128)S(1)} %copy-done.5), custom_call_target="tpu_custom_call" | custom-call | tf_op jit(solution)/shard_map/pallas_call | solution.py:585
  82.9 0.8 copy.8
Async XLA Ops:
  0.0 1.6 %copy-start = (bf16[512,2048]{1,0:T(8,128)(2,1)S(1)}, bf16[512,2048]{1,0:T(8,128)(2,1)}, u32[]{:S(2)}) copy-start(bf16[512,2048]{1,0:T(8,128)(2,1)} %tokens.1) | copy-start | bytes 6291460
  1.6 0.9 %copy-start.1 = (bf16[256,384]{1,0:T(8,128)(2,1)S(1)}, bf16[256,384]{1,0:T(8,128)(2,1)}, u32[]{:S(2)}) copy-start(bf16[256,384]{1,0:T(8,128)(2,1)} %w_key.1) | copy-start | bytes 589828
  2.5 0.9 %copy-start.2 = (bf16[256,384]{1,0:T(8,128)(2,1)S(1)}, bf16[256,384]{1,0:T(8,128)(2,1)}, u32[]{:S(2)}) copy-start(bf16[256,384]{1,0:T(8,128)(2,1)} %w_value.1) | copy-start | bytes 589828
  3.4 0.9 %copy-start.3 = (bf16[256,384]{1,0:T(8,128)(2,1)S(1)}, bf16[256,384]{1,0:T(8,128)(2,1)}, u32[]{:S(2)}) copy-start(bf16[256,384]{1,0:T(8,128)(2,1)} %w_query.1) | copy-start | bytes 589828
  4.4 0.8 %copy-start.4 = (bf16[128,256]{1,0:T(8,128)(2,1)S(1)}, bf16[128,256]{1,0:T(8,128)(2,1)}, u32[]{:S(2)}) copy-start(bf16[128,256]{1,0:T(8,128)(2,1)} %w_out.1) | copy-start | bytes 196612
  5.2 0.7 copy-start.5
where the time goes:
time: 84 us; the launch traced here: 83.7 us
  Pallas kernels  77 us (92%)
  local copies, waits for them, and re-layouts  6.66 us (8%)
    pallas_call x1, Pallas kernels, one_kernel(): pl.pallas_call(functools.partial(layer_kernel, nz), out_shape=jax.ShapeDt...  77 us
    unnamed x13, local copies, waits for them, and re-layouts  6.66 us

commit v1 on v0

--- a/solution.py
+++ b/solution.py
@@ -3,7 +3,6 @@
 
 import jax
 import jax.numpy as jnp
-import numpy as np
 from jax import lax
 from jax.experimental import pallas as pl
 from jax.experimental.pallas import tpu as pltpu
@@ -159,7 +158,7 @@
 
 def layer_kernel(
     nz,
-    tokens, w_key, w_value, w_query, w_out, freq, out,
+    tokens, w_key, w_value, w_query, w_out, out,
     weights, tok_in, tok_turned, cosine, sine, queries, pair0, send1, near1, far2,
     out_rows, mine, heads_in, got01, top01, sum01,
     swap_s, tok_r, w_r, up_s, down_s, side_s, o_r, o_s, o_r2, far_s, far_r, near_s, near_r, head_s, head_r,
@@ -187,6 +186,38 @@
             device_id=where, device_id_type=pl.DeviceIdType.MESH,
         )
 
+    parts = (w_key, w_value, w_query)
+
+    def chunk(a, s):
+        return weights.at[a, pl.ds(pl.multiple_of(s * k_rows, k_rows), k_rows), :]
+
+    def o_chunk(zz):
+        return out_rows.at[c, x, y, zz]
+
+    def swapped(a):
+        there = 2 * z + 1 - c
+        return send(parts[a], chunk(a, there), swap_s.at[a], w_r.at[a, there], partner)
+
+    def tok_swapped():
+        return send(tokens, tok_in, swap_s.at[3], tok_r, partner)
+
+    def kept(a):
+        return pltpu.make_async_copy(parts[a], chunk(a, rank), w_r.at[a, rank])
+
+    def o_kept():
+        return pltpu.make_async_copy(w_out, o_chunk(z), o_r.at[z])
+
+    def tok_kept():
+        return pltpu.make_async_copy(tokens, tok_in, tok_r)
+
+    @pl.when(stays)
+    def _():
+        for a in range(3):
+            kept(a).start()
+        tok_kept().start()
+
+    o_kept().start()
+
     barrier = pltpu.get_barrier_semaphore()
 
     def greet(where):
@@ -204,40 +235,12 @@
     greeters = 7 + jnp.where(has_up, 1 + c, 0) + jnp.where(has_down, 2 - c, 0)
     pl.semaphore_wait(barrier, greeters)
 
-    parts = (w_key, w_value, w_query)
-
-    def chunk(a, s):
-        return weights.at[a, pl.ds(pl.multiple_of(s * k_rows, k_rows), k_rows), :]
-
-    def o_chunk(zz):
-        return out_rows.at[c, x, y, zz]
-
-    def swapped(a):
-        there = 2 * z + 1 - c
-        return send(parts[a], chunk(a, there), swap_s.at[a], w_r.at[a, there], partner)
-
-    def tok_swapped():
-        return send(tokens, tok_in, swap_s.at[3], tok_r, partner)
-
-    def kept(a):
-        return pltpu.make_async_copy(parts[a], chunk(a, rank), w_r.at[a, rank])
-
-    def o_kept():
-        return pltpu.make_async_copy(w_out, o_chunk(z), o_r.at[z])
-
-    @pl.when(stays)
-    def _():
-        for a in range(3):
-            kept(a).start()
-
     @pl.when(jnp.logical_not(stays))
     def _():
         swapped(0).start()
         swapped(1).start()
         tok_swapped().start()
         swapped(2).start()
-
-    o_kept().start()
 
     def go(a, zz, kind):
         s = 2 * zz + c
@@ -289,10 +292,13 @@
     own(0)
     own(1)
 
+    pair_at = lax.broadcasted_iota(jnp.int32, (1, DH), 1) & (DH // 2 - 1)
+    freq = jnp.exp(pair_at.astype(jnp.float32) * (-2.0 * math.log(ROPE_BASE) / DH))
+
     def angles(index, carry):
         rows = pl.ds(pl.multiple_of(index * block, block), block)
         p = lax.broadcasted_iota(jnp.int32, (block, DH), 0) + index * block
-        angle = (row_time(p) + rank * tok_rows).astype(jnp.float32) * freq[...]
+        angle = (row_time(p) + rank * tok_rows).astype(jnp.float32) * freq
         lane = lax.broadcasted_iota(jnp.int32, (block, DH), 1)
         cosine[rows, :] = jnp.cos(angle)
         turned = jnp.sin(angle)
@@ -321,7 +327,10 @@
 
         lax.fori_loop(0, depth // 256, piece, 0)
 
-    pl.when(stays)(lambda: order(tokens))
+    @pl.when(stays)
+    def _():
+        tok_kept().wait()
+        order(tok_in)
 
     def o_y():
         return send(out_rows.at[c, x, y], out_rows.at[c, x, y], o_s.at[0], o_r2.at[0], (2 * z + 1 - y, tp))
@@ -385,10 +394,10 @@
         return send(send1, near1, near_s, near_r, where)
 
     up_other = (sp + 2, 2 * x)
+    pl.when(has_up & (c == 1))(lambda: near(up_other).start())
     pl.when(has_up)(lambda: far(0, 0, 2, above).start())
+    pl.when(c == 0)(lambda: near(side).start())
     pl.when(c == 0)(lambda: far(1, 0, 1, side).start())
-    pl.when(c == 0)(lambda: near(side).start())
-    pl.when(has_up & (c == 1))(lambda: near(up_other).start())
 
     for d in range(1, 5):
         @pl.when(rank < d)
@@ -579,13 +588,11 @@
     nz = n_sp // 2
     tok_rows, depth = tokens.shape
     cols = w_query.shape[1]
-    half = 1.0 / ROPE_BASE ** (np.arange(0, DH, 2) / DH)
-    freq = jnp.asarray(np.concatenate([half, half]).reshape(1, DH), jnp.float32)
     bf, dma = jnp.bfloat16, pltpu.SemaphoreType.DMA
     return pl.pallas_call(
         functools.partial(layer_kernel, nz),
         out_shape=jax.ShapeDtypeStruct((tok_rows // 4, w_out.shape[1] * n_sp), bf),
-        in_specs=[pl.BlockSpec(memory_space=pltpu.VMEM)] * 6,
+        in_specs=[pl.BlockSpec(memory_space=pltpu.HBM)] * 5,
         out_specs=pl.BlockSpec(memory_space=pltpu.VMEM),
         scratch_shapes=[
             pltpu.VMEM((3, depth, cols), bf),
@@ -611,9 +618,9 @@
             dma((4,)), dma((4,)),
         ],
         compiler_params=pltpu.CompilerParams(
-            collective_id=0, has_side_effects=True, vmem_limit_bytes=32 * 1024 * 1024
+            collective_id=0, has_side_effects=True, vmem_limit_bytes=60 * 1024 * 1024
         ),
-    )(tokens, w_key, w_value, w_query, w_out, freq)
+    )(tokens, w_key, w_value, w_query, w_out)
 
 
 def on_mesh(n_sp, n_tp, *operands):

time: 84 us -> 78.9 us (0.939)
  local copies, waits for them, and re-layouts: 6.66 us -> 1.88 us
    unnamed x13 -> x1, local copies, waits for them, and re-layouts: 6.66 us -> 1.88 us
where the time goes in v1:
time: 78.9 us; the launch traced here: 78.7 us
  Pallas kernels  76.8 us (97%)
  local copies, waits for them, and re-layouts  1.88 us (2%)
    pallas_call x1, Pallas kernels, one_kernel(): pl.pallas_call(functools.partial(layer_kernel, nz), out_shape=jax.ShapeDt...  76.8 us
    unnamed x1, local copies, waits for them, and re-layouts  1.88 us

profile of v1, /device:TPU:25, one launch (start us, length us, event | category | flops | bytes accessed | tf_op | source)
XLA Modules:
  0.0 78.7 jit_solution(5317819443790387477)
XLA Ops:
  0.0 76.8 %shard_map.55 = bf16[128,2048]{1,0:T(8,128)(2,1)} custom-call(bf16[512,2048]{1,0:T(8,128)(2,1)} %tokens.1, bf16[256,384]{1,0:T(8,128)(2,1)} %w_key.1, bf16[256,384]{1,0:T(8,128)(2,1)} %w_value.1, bf16[256,384]{1,0:T(8,128)(2,1)} %w_query.1, bf16[128,256]{1,0:T(8,128)(2,1)} %w_out.1), custom_call_target="tpu_custom_call" | custom-call | tf_op jit(solution)/shard_map/pallas_call | solution.py:592
  76.8 1.9 %copy.7 = bf16[128,2048]{1,0:T(8,128)(2,1)} copy(bf16[128,2048]{1,0:T(8,128)(2,1)} %shard_map.55) | data formatting | bytes 1048576

commit v2 on v1

--- a/solution.py
+++ b/solution.py
@@ -384,6 +384,8 @@
 
     others(0)
     project(0, keep_pair(0))
+    if nz > 2:
+        relay(2, 2)
     others(1)
     project(1, keep_pair(1))
 
@@ -408,7 +410,7 @@
     def _():
         near1[...] = jnp.zeros(near1.shape, near1.dtype)
 
-    for d in range(2, nz):
+    for d in range(3, nz):
         relay(2, d)
     @pl.when(has_down)
     def _():
@@ -474,29 +476,37 @@
         sum01[rows, :] = f0 * sum0 + f1 * sum1
         return carry
 
-    def far_group(index, carry):
+    def far_group(slots, last, index, carry):
         begin = index * block
         rows = pl.ds(pl.multiple_of(begin, block), block)
+        heres = [pl.ds(pl.multiple_of(begin + b * sub, sub), sub) for b in range(4)]
         all_scores = []
-        for b in range(4):
-            here = pl.ds(pl.multiple_of(begin + b * sub, sub), sub)
-            keys = jnp.concatenate([far2[d, 0, here, :] for d in (4, 3, 2, 1, 0)], axis=0)
+        for here in heres:
+            keys = jnp.concatenate([far2[d, 0, here, :] for d in slots], axis=0)
             all_scores.append(dots(queries[2, here, :], keys))
         scores = jnp.concatenate(all_scores, axis=0)
-        step_q = iota((block, 1), 0) & (sub - 1)
-        step_k = iota((1, 5 * sub), 1) - 4 * sub
-        top2, sum2, weight = soft(scores, step_q, step_k, WIN3 // THIRD_DILATION, -rank * sub)
+        time_q = iota((block, 1), 0) & (sub - 1)
+        time_k = iota((1, len(slots) * sub), 1) - slots[0] * sub
+        gap = time_q - jnp.where(time_k >= -rank * sub, time_k, far_off)
+        allowed = (gap >= 0) & (gap <= WIN3 // THIRD_DILATION)
+        scores = jnp.where(allowed, scores * scale, -jnp.inf)
+        before = top01[rows, :]
+        top = jnp.maximum(before, jnp.max(scores, axis=-1, keepdims=True))
+        factor = jnp.exp(before - top)
+        weight = jnp.exp(scores - top)
+        total = factor * sum01[rows, :] + jnp.sum(weight, axis=-1, keepdims=True)
+        weight = weight.astype(jnp.bfloat16)
         got = []
-        for b in range(4):
-            here = pl.ds(pl.multiple_of(begin + b * sub, sub), sub)
-            vals = jnp.concatenate([far2[d, 1, here, :] for d in (4, 3, 2, 1, 0)], axis=0)
+        for b, here in enumerate(heres):
+            vals = jnp.concatenate([far2[d, 1, here, :] for d in slots], axis=0)
             got.append(jnp.dot(weight[b * sub : (b + 1) * sub], vals, preferred_element_type=jnp.float32))
-        got2 = jnp.concatenate(got, axis=0)
-        top1 = top01[rows, :]
-        top = jnp.maximum(top1, top2)
-        f1, f2 = jnp.exp(top1 - top), jnp.exp(top2 - top)
-        total = f1 * sum01[rows, :] + f2 * sum2
-        mine[0, rows, :] = ((f1 * got01[rows, :] + f2 * got2) / total).astype(jnp.bfloat16)
+        both = factor * got01[rows, :] + jnp.concatenate(got, axis=0)
+        if last:
+            mine[0, rows, :] = (both / total).astype(jnp.bfloat16)
+        else:
+            got01[rows, :] = both
+            top01[rows, :] = top
+            sum01[rows, :] = total
         return carry
 
     pl.when(rank >= 1)(lambda: near(side).wait_recv())
@@ -504,14 +514,16 @@
     o_x().wait()
     o_c().start()
 
+    pl.when(rank >= 1)(lambda: far(1, 0, 1, side).wait_recv())
+    lax.fori_loop(0, SECOND_DILATION, functools.partial(far_group, (2, 1, 0), False), 0)
+
     @pl.when(z >= 2)
     def _():
         far(2, 2, 4, above).wait_recv()
         pl.when(c == 1)(lambda: far(4, 4, 3, side).start())
 
-    pl.when(rank >= 1)(lambda: far(1, 0, 1, side).wait_recv())
     pl.when(rank >= 3)(lambda: far(4, 4, 3, side).wait_recv())
-    lax.fori_loop(0, SECOND_DILATION, far_group, 0)
+    lax.fori_loop(0, SECOND_DILATION, functools.partial(far_group, (4, 3), True), 0)
 
     t = iota((tok_rows, tok_rows), 0)
     p = row_time(iota((tok_rows, tok_rows), 1))

time: 78.9 us -> 78.9 us (level)
  no operation moved by 1% of the time
where the time goes in v2:
time: 78.9 us; the launch traced here: 78.8 us
  Pallas kernels  76.9 us (97%)
  local copies, waits for them, and re-layouts  1.88 us (2%)
    pallas_call x1, Pallas kernels, one_kernel(): pl.pallas_call(functools.partial(layer_kernel, nz), out_shape=jax.ShapeDt...  76.9 us
    unnamed x1, local copies, waits for them, and re-layouts  1.88 us

profile of v2, /device:TPU:25, one launch (start us, length us, event | category | flops | bytes accessed | tf_op | source)
XLA Modules:
  0.0 78.8 jit_solution(16405939627872964184)
XLA Ops:
  0.0 76.9 %shard_map.55 = bf16[128,2048]{1,0:T(8,128)(2,1)} custom-call(bf16[512,2048]{1,0:T(8,128)(2,1)} %tokens.1, bf16[256,384]{1,0:T(8,128)(2,1)} %w_key.1, bf16[256,384]{1,0:T(8,128)(2,1)} %w_value.1, bf16[256,384]{1,0:T(8,128)(2,1)} %w_query.1, bf16[128,256]{1,0:T(8,128)(2,1)} %w_out.1), custom_call_target="tpu_custom_call" | custom-call | tf_op jit(solution)/shard_map/pallas_call | solution.py:604
  76.9 1.9 %copy.7 = bf16[128,2048]{1,0:T(8,128)(2,1)} copy(bf16[128,2048]{1,0:T(8,128)(2,1)} %shard_map.55) | data formatting | bytes 1048576
